TPU v7x, 32 devices: a whole 2x2x4 slice. The times are simulated.
32 devices in a mesh: ep: 8 (over z, y), tp: 4 (over x, core).
Axes of the slice: x: 2, y: 2, z: 4, core: 2. Of those that a mesh axis runs over, the one named last changes fastest.
Arguments:
- tokens: bfloat16 [2048, 2048], P('ep'), may hold values from -6 to 6
- norm_gain: float32 [2048], replicated, may hold values from 0.1 to 1.9
- expert_ids: int32 [2048, 2], P('ep'), may hold values from 0 to 3, all different within a row; in each aligned block of 256 rows (0 to 255, 256 to 511, ...) at most 160 rows name the same one
- route_weight: float32 [2048, 2], P('ep'), may hold values from 0.2 to 1
- w_gate: bfloat16 [8, 2048, 3584], P('ep', None, 'tp'), may hold values from -0.125 to 0.125
- w_up: bfloat16 [8, 2048, 3584], P('ep', None, 'tp'), may hold values from -0.125 to 0.125
- w_down: bfloat16 [8, 3584, 2048], P('ep', 'tp'), may hold values from -0.0625 to 0.0625
Outputs:
- mixed: bfloat16 [2048, 2048], P('ep', 'tp')
Inputs may be any that keep to these rules, and one draw needn't show every extreme that they name: `expert_ids`: A token names 2 different experts. In each aligned block of 256 tokens (the tokens of one index of ep) no expert is named by more than 160 tokens, a bound that some block reaches.
All inputs are finite; a program needn't handle non-finite values.
Results may differ from a plain program's by a relative error of at most 0.014.
Values may be sent and summed in bfloat16 or wider, within the bound.
A program may use at most 128 MiB of HBM per device.

v0:
```python
import jax
import jax.numpy as jnp
from jax import lax
from jax.sharding import PartitionSpec as P

HALVES = 2
EPSILON = 1e-05


def layer_normed(tokens, norm_gain):
    values = tokens.astype(jnp.float32)
    center = values - jnp.mean(values, axis=-1, keepdims=True)
    spread = jnp.mean(center * center, axis=-1, keepdims=True)
    return (center * lax.rsqrt(spread + EPSILON) * norm_gain).astype(jnp.bfloat16)


def slot_numbers(chosen, experts):
    onehot = (chosen[..., None] == jnp.arange(experts, dtype=jnp.int32)).astype(jnp.int32)
    before = jnp.cumsum(onehot, axis=1) - onehot
    return jnp.sum(before * onehot, axis=-1)


def body(tokens, norm_gain, expert_ids, route_weight, w_gate, w_up, w_down):
    tok_rows, width = tokens.shape
    top_count = expert_ids.shape[1]
    ep_count = lax.axis_size("ep")
    experts = ep_count // HALVES
    capacity = 2 * min(tok_rows // 2, 5 * tok_rows * top_count // (8 * experts))
    normed = layer_normed(tokens, norm_gain)
    padded = jnp.concatenate([normed, jnp.zeros((1, width), jnp.bfloat16)], axis=0)
    slots = slot_numbers(expert_ids.reshape(1, -1), experts).reshape(-1)
    flat_expert = expert_ids.reshape(-1)
    owner = jnp.arange(tok_rows * top_count, dtype=jnp.int32) // top_count
    place = flat_expert * capacity + slots
    table = jnp.full((experts * capacity,), tok_rows, jnp.int32).at[place].set(owner)
    outgoing = padded[table].reshape(experts, capacity, width)
    columns = width // lax.axis_size("tp")
    portion = lax.dynamic_slice_in_dim(outgoing, lax.axis_index("tp") * columns, columns, 2)
    doubled = jnp.repeat(portion, HALVES, axis=0)
    pieces = lax.all_to_all(doubled, "ep", split_axis=0, concat_axis=0, tiled=True)
    arrived = lax.all_gather(pieces, "tp", axis=2, tiled=True)
    routed = arrived.reshape(-1, width)
    gate = jnp.dot(routed, w_gate[0], preferred_element_type=jnp.float32)
    up = jnp.dot(routed, w_up[0], preferred_element_type=jnp.float32)
    hidden = (jax.nn.silu(gate) * up).astype(jnp.bfloat16)
    partial_value = jnp.dot(hidden, w_down[0], preferred_element_type=jnp.float32)
    reduced = lax.psum_scatter(
        partial_value.astype(jnp.bfloat16), "tp", scatter_dimension=1, tiled=True
    )
    returned = lax.all_to_all(
        reduced.reshape(ep_count, capacity, -1), "ep", split_axis=0, concat_axis=0, tiled=True
    )
    quarter = returned.shape[2]
    summed = returned.reshape(experts, HALVES, capacity, quarter).astype(jnp.float32).sum(axis=1)
    picked = summed.reshape(experts * capacity, quarter)[place].reshape(
        tok_rows, top_count, quarter
    )
    mixed = jnp.sum(route_weight[:, :, None] * picked, axis=1)
    return mixed.astype(jnp.bfloat16)


def solution(mesh):
    return jax.shard_map(
        body,
        mesh=mesh,
        in_specs=(
            P("ep", None),
            P(),
            P("ep", None),
            P("ep", None),
            P("ep", None, "tp"),
            P("ep", None, "tp"),
            P("ep", "tp", None),
        ),
        out_specs=P("ep", "tp"),
        check_vma=False,
    )
```

profile of v0, /device:TPU:0, one launch (start us, length us, event | category | flops | bytes accessed | tf_op | source)
XLA Modules:
  0.0 228.1 jit_solution(8858825932461723816)
XLA Ops:
  6.5 0.8 copy.11
  7.4 0.1 eq.27
  7.5 1.2 reduce-window.6
  8.8 0.2 slice_reduce_fusion
  9.0 0.7 broadcast_multiply_fusion
  9.7 0.2 reduce-window.9
  10.1 0.1 mul.64
  10.3 2.4 %scatter_custom_fusion = s32[640]{0:T(1024)S(1)} fusion(s32[512]{0:T(512)S(1)} %bitcast.41, s32[512]{0:T(512)S(1)} %add_select_fusion, s32[]{:T(128)} %constant.41.clone.1), kind=kCustom, calls=%fused_computation.35 | custom fusion | bytes 2564 | tf_op jit(solution)/shard_map/scatter | solution.py:35
  12.8 1.4 convert_reduce_fusion
  14.2 1.6 fusion.6
  15.9 1.6 fusion.8
  17.6 4.1 %gather_fusion = bf16[640,2048]{1,0:T(8,128)(2,1)} fusion(bf16[257,2048]{1,0:T(8,128)(2,1)S(1)} %concatenate.3, s32[1024]{0:T(1024)S(1)} %pad_clamp_fusion.1), kind=kCustom, calls=%fused_computation | custom fusion | bytes 5245440 | tf_op jit(solution)/shard_map/gather | solution.py:36
  21.7 1.1 constant_dynamic-slice_fusion
  22.9 38.6 %all_to_all.10 = bf16[8,160,512]{2,1,0:T(8,128)(2,1)} all-to-all(bf16[8,160,512]{2,1,0:T(8,128)(2,1)S(1)} %bitcast.38), channel_id=1, replica_groups=mesh['ep'=8,'tp'=4] {'ep'}, dimensions={0} | all-to-all | bytes 2621440 | tf_op jit(solution)/shard_map/all_to_all | solution.py:40
  61.6 39.5 %all-gather.2.cloned.1.call-done = bf16[8,160,2048]{2,1,0:T(8,128)(2,1)} async-done(((bf16[8,160,512]{2,1,0:T(8,128)(2,1)}), bf16[8,160,2048]{2,1,0:T(8,128)(2,1)}) %all-gather.2.cloned.1.call-update) | async-done | bytes 5242896 | tf_op jit(solution)/shard_map/all_gather | solution.py:41
  101.1 10.0 %fusion.2 = f32[1280,896]{1,0:T(8,128)} fusion(bf16[1280,2048]{1,0:T(8,128)(2,1)} %bitcast.45, bf16[1,2048,896]{2,1,0:T(8,128)(2,1)} %param.11), kind=kOutput, calls=%fused_computation.7 | convolution fusion | flops 4697620480 | bytes 13500416 | tf_op jit(solution)/shard_map/dot_general | solution.py:43
  111.1 17.6 %convolution_convert_fusion = bf16[1280,2048]{1,0:T(8,128)(2,1)} fusion(bf16[1,896,2048]{2,1,0:T(8,128)(2,1)} %param.13, f32[1280,896]{1,0:T(8,128)} %fusion.2, bf16[1280,2048]{1,0:T(8,128)(2,1)} %bitcast.46, bf16[1,2048,896]{2,1,0:T(8,128)(2,1)} %param.12), kind=kOutput, calls=%fused_computation.3 | convolution fusion | flops 9404743680 | bytes 22413312 | tf_op jit(solution)/shard_map/dot_general | solution.py:46
  128.7 51.3 %reduce-scatter.2.cloned.1.call-done = bf16[1280,512]{1,0:T(8,128)(2,1)} async-done(((bf16[1280,2048]{1,0:T(8,128)(2,1)}), bf16[1280,512]{1,0:T(8,128)(2,1)}) %reduce-scatter.2.cloned.1.call-update) | async-done | bytes 1310736 | tf_op jit(solution)/shard_map/reduce_scatter | solution.py:47
  180.0 5.5 %all-to-all-start.1 = ((bf16[8,160,512]{2,1,0:T(8,128)(2,1)}), bf16[8,160,512]{2,1,0:T(8,128)(2,1)S(1)}, u32[]{:S(2)}, u32[]{:S(2)}) async-start(bf16[8,160,512]{2,1,0:T(8,128)(2,1)} %bitcast.40), calls=%async_computation.2 | async-start | bytes 2621440 | tf_op jit(solution)/shard_map/all_to_all | solution.py:50
  185.7 31.1 %all-to-all-done.1 = bf16[8,160,512]{2,1,0:T(8,128)(2,1)S(1)} async-done(((bf16[8,160,512]{2,1,0:T(8,128)(2,1)}), bf16[8,160,512]{2,1,0:T(8,128)(2,1)S(1)}, u32[]{:S(2)}, u32[]{:S(2)}) %all-to-all-start.1) | async-done | bytes 1310752 | tf_op jit(solution)/shard_map/all_to_all | solution.py:50
  216.7 0.2 convert_reduce_fusion.1
  216.9 1.6 gather_fusion.1
  218.6 0.6 reshape.191
  219.2 2.1 multiply_reduce_fusion
  (24 shorter events, 0.7 us)
Async XLA Ops:
  6.5 94.6 %all-gather.2.cloned.1.call-start = ((), (), s32[]{:S(2)}) async-start(), calls=%async_computation.3 | async-start | bytes 6553600 | tf_op jit(solution)/shard_map/all_gather | solution.py:41
  61.5 118.4 %reduce-scatter.2.cloned.1.call-start = ((), (), s32[]{:S(2)}) async-start(), calls=%async_computation.4 | async-start | bytes 6553600 | tf_op jit(solution)/shard_map/reduce_scatter | solution.py:47
  128.6 56.9 %copy-start = (f32[256,2]{0,1:T(2,128)S(1)}, f32[256,2]{0,1:T(2,128)}, u32[]{:S(2)}) copy-start(f32[256,2]{0,1:T(2,128)} %param.10) | copy-start | bytes 6148
  180.0 36.7 %all-to-all-start.1 = ((bf16[8,160,512]{2,1,0:T(8,128)(2,1)}), bf16[8,160,512]{2,1,0:T(8,128)(2,1)S(1)}, u32[]{:S(2)}, u32[]{:S(2)}) async-start(bf16[8,160,512]{2,1,0:T(8,128)(2,1)} %bitcast.40), calls=%async_computation.2 | async-start | bytes 2621440 | tf_op jit(solution)/shard_map/all_to_all | solution.py:50
Sparse Core Ops, SparseCore 0:
  61.7 39.4 all-gather.1
  128.8 51.1 reduce-scatter.1
where the time goes:
time: 228 us
  waiting for transfers between devices  122 us (54%)
  blocking collectives  38.6 us (17%)
  matrix products  27.5 us (12%)
  between operations  13.6 us (6%)
  local copies, waits for them, and re-layouts  11.8 us (5%)
  other arithmetic  9.14 us (4%)
  starting transfers between devices  5.56 us (2%)
    reduce_scatter x1, waiting for transfers between devices, body(): lax.psum_scatter(partial_value.astype(jnp.bfloat16), 'tp', scatter_dimens...  51.3 us
    all_gather x1, waiting for transfers between devices, body(): arrived = lax.all_gather(pieces, 'tp', axis=2, tiled=True)  39.5 us
    all_to_all x1, blocking collectives, body(): lax.all_to_all(doubled, 'ep', split_axis=0, concat_axis=0, tiled=True)  38.6 us
    all_to_all x1, waiting for transfers between devices, body(): lax.all_to_all(reduced.reshape(ep_count, capacity, -1), 'ep', split_axis=...  31.1 us
    dot_general x1, matrix products, body(): jnp.dot(hidden, w_down[0], preferred_element_type=jnp.float32)  17.6 us
    dot_general x1, matrix products, body(): gate = jnp.dot(routed, w_gate[0], preferred_element_type=jnp.float32)  9.98 us
    all_to_all x1, starting transfers between devices, body(): lax.all_to_all(reduced.reshape(ep_count, capacity, -1), 'ep', split_axis=...  5.52 us
  transfers between devices with their start and end apart: 3, of which 3 were waited for; matrix products, arithmetic and copies ran while one was open for 0% of the time, Pallas kernels for 0%

commit v1 on v0

--- a/solution.py
+++ b/solution.py
@@ -38,7 +38,9 @@
     portion = lax.dynamic_slice_in_dim(outgoing, lax.axis_index("tp") * columns, columns, 2)
     doubled = jnp.repeat(portion, HALVES, axis=0)
     pieces = lax.all_to_all(doubled, "ep", split_axis=0, concat_axis=0, tiled=True)
-    arrived = lax.all_gather(pieces, "tp", axis=2, tiled=True)
+    arrived = jnp.concatenate(
+        lax.all_to_all(jnp.stack([pieces] * lax.axis_size("tp")), "tp", 0, 0), axis=2
+    )
     routed = arrived.reshape(-1, width)
     gate = jnp.dot(routed, w_gate[0], preferred_element_type=jnp.float32)
     up = jnp.dot(routed, w_up[0], preferred_element_type=jnp.float32)

time: 228 us -> 255 us (1.12)
  blocking collectives: 38.6 us -> 100 us
  waiting for transfers between devices: 122 us -> 80.5 us
  local copies, waits for them, and re-layouts: 11.8 us -> 21.1 us
  matrix products: 27.5 us -> 24.7 us
    all_to_all x0 -> x1, blocking collectives: none -> 62 us  [body(): lax.all_to_all(jnp.stack([pieces] * lax.axis_size('tp')), 'tp', 0, 0)]
    all_gather x1 -> x0, waiting for transfers between devices: 39.5 us -> none  [body(): arrived = lax.all_gather(pieces, 'tp', axis=2, tiled=True)]
    unnamed x4 -> x9, local copies, waits for them, and re-layouts: 0.94 us -> 5.56 us
    reshape x1 -> x2, local copies, waits for them, and re-layouts: 0.02 us -> 4.07 us  [the longest x1 4.05 us: body(): jnp.concatenate(lax.all_to_all(jnp.stack([pieces] * lax.axis_size('tp')),...]
    dot_general x1, matrix products: 9.98 us -> 7.15 us  [body(): gate = jnp.dot(routed, w_gate[0], preferred_element_type=jnp.float32)]
  transfers between devices with their start and end apart: 3 -> 2, of which waited for: 3 -> 2; matrix products, arithmetic and copies ran while one was open for 0% -> 0% of each run, Pallas kernels for 0% -> 0%
where the time goes in v1:
time: 255 us
  blocking collectives  100 us (39%)
  waiting for transfers between devices  80.5 us (32%)
  matrix products  24.7 us (10%)
  local copies, waits for them, and re-layouts  21.1 us (8%)
  between operations  13.6 us (5%)
  other arithmetic  9.14 us (4%)
  starting transfers between devices  5.53 us (2%)
    all_to_all x1, blocking collectives, body(): lax.all_to_all(jnp.stack([pieces] * lax.axis_size('tp')), 'tp', 0, 0)  62 us
    reduce_scatter x1, waiting for transfers between devices, body(): lax.psum_scatter(partial_value.astype(jnp.bfloat16), 'tp', scatter_dimens...  49.4 us
    all_to_all x1, blocking collectives, body(): lax.all_to_all(doubled, 'ep', split_axis=0, concat_axis=0, tiled=True)  38.5 us
    all_to_all x1, waiting for transfers between devices, body(): lax.all_to_all(reduced.reshape(ep_count, capacity, -1), 'ep', split_axis=...  31.1 us
    dot_general x1, matrix products, body(): jnp.dot(hidden, w_down[0], preferred_element_type=jnp.float32)  17.5 us
    dot_general x1, matrix products, body(): gate = jnp.dot(routed, w_gate[0], preferred_element_type=jnp.float32)  7.15 us
    unnamed x9, local copies, waits for them, and re-layouts  5.56 us
    all_to_all x1, starting transfers between devices, body(): lax.all_to_all(reduced.reshape(ep_count, capacity, -1), 'ep', split_axis=...  5.52 us
  transfers between devices with their start and end apart: 2, of which 2 were waited for; matrix products, arithmetic and copies ran while one was open for 0% of the time, Pallas kernels for 0%

profile of v1, /device:TPU:0, one launch (start us, length us, event | category | flops | bytes accessed | tf_op | source)
XLA Modules:
  0.0 255.0 jit_solution(7795269746719498098)
XLA Ops:
  6.5 0.8 copy.14
  7.5 1.2 reduce-window.6
  9.0 0.7 broadcast_multiply_fusion
  10.3 2.4 scatter_custom_fusion
  12.8 1.4 convert_reduce_fusion
  14.2 1.6 fusion.6
  15.9 1.6 fusion.8
  17.6 4.1 %gather_fusion = bf16[640,2048]{1,0:T(8,128)(2,1)} fusion(bf16[257,2048]{1,0:T(8,128)(2,1)S(1)} %concatenate.3, s32[1024]{0:T(1024)S(1)} %pad_clamp_fusion.1), kind=kCustom, calls=%fused_computation | custom fusion | bytes 5245440 | tf_op jit(solution)/shard_map/gather | solution.py:36
  21.7 1.1 constant_dynamic-slice_fusion
  22.9 38.5 %all_to_all.15 = bf16[8,160,512]{2,1,0:T(8,128)(2,1)S(1)} all-to-all(bf16[8,160,512]{2,1,0:T(8,128)(2,1)S(1)} %bitcast.45), channel_id=1, replica_groups=mesh['ep'=8,'tp'=4] {'ep'}, dimensions={0} | all-to-all | bytes 2621440 | tf_op jit(solution)/shard_map/all_to_all | solution.py:40
  61.4 0.6 stack.2
  62.1 62.0 %all_to_all.16 = bf16[4,8,160,512]{3,2,1,0:T(8,128)(2,1)S(1)} all-to-all(bf16[4,8,160,512]{3,2,1,0:T(8,128)(2,1)S(1)} %stack.2), channel_id=1, replica_groups=mesh['ep'=8,'tp'=4] {'tp'}, dimensions={0} | all-to-all | bytes 10485760 | tf_op jit(solution)/shard_map/all_to_all | solution.py:42
  124.0 4.1 %copy.15 = bf16[8,160,4,512]{3,2,1,0:T(4,128)(2,1)S(1)} copy(bf16[8,160,4,512]{3,1,0,2:T(8,128)(2,1)S(1)} %bitcast.41) | data formatting | bytes 10485760 | tf_op jit(solution)/shard_map/reshape | solution.py:41
  128.1 2.3 copy.16
  130.4 2.3 copy-done
  132.7 7.1 %fusion.2 = f32[1280,896]{1,0:T(8,128)} fusion(bf16[1280,2048]{1,0:T(8,128)(2,1)S(1)} %bitcast.43, bf16[1,2048,896]{2,1,0:T(8,128)(2,1)S(1)} %copy-done.2), kind=kOutput, calls=%fused_computation.7 | convolution fusion | flops 4697620480 | bytes 13500416 | tf_op jit(solution)/shard_map/dot_general | solution.py:45
  139.9 17.5 %convolution_convert_fusion = bf16[1280,2048]{1,0:T(8,128)(2,1)} fusion(bf16[1,896,2048]{2,1,0:T(8,128)(2,1)} %param.13, f32[1280,896]{1,0:T(8,128)} %fusion.2, bf16[1280,2048]{1,0:T(8,128)(2,1)} %bitcast.44, bf16[1,2048,896]{2,1,0:T(8,128)(2,1)} %param.12), kind=kOutput, calls=%fused_computation.3 | convolution fusion | flops 9404743680 | bytes 22413312 | tf_op jit(solution)/shard_map/dot_general | solution.py:48
  157.4 49.4 %reduce-scatter.2.cloned.1.call-done = bf16[1280,512]{1,0:T(8,128)(2,1)} async-done(((bf16[1280,2048]{1,0:T(8,128)(2,1)}), bf16[1280,512]{1,0:T(8,128)(2,1)}) %reduce-scatter.2.cloned.1.call-update) | async-done | bytes 1310736 | tf_op jit(solution)/shard_map/reduce_scatter | solution.py:49
  206.8 5.5 %all-to-all-start.2 = ((bf16[8,160,512]{2,1,0:T(8,128)(2,1)}), bf16[8,160,512]{2,1,0:T(8,128)(2,1)S(1)}, u32[]{:S(2)}, u32[]{:S(2)}) async-start(bf16[8,160,512]{2,1,0:T(8,128)(2,1)} %bitcast.47), calls=%async_computation.3 | async-start | bytes 2621440 | tf_op jit(solution)/shard_map/all_to_all | solution.py:52
  212.5 31.1 %all-to-all-done.2 = bf16[8,160,512]{2,1,0:T(8,128)(2,1)S(1)} async-done(((bf16[8,160,512]{2,1,0:T(8,128)(2,1)}), bf16[8,160,512]{2,1,0:T(8,128)(2,1)S(1)}, u32[]{:S(2)}, u32[]{:S(2)}) %all-to-all-start.2) | async-done | bytes 1310752 | tf_op jit(solution)/shard_map/all_to_all | solution.py:52
  243.6 0.2 convert_reduce_fusion.1
  243.8 1.6 gather_fusion.1
  245.4 0.6 reshape.193
  246.1 2.1 multiply_reduce_fusion
  (29 shorter events, 1.4 us)
Async XLA Ops:
  6.5 200.3 %reduce-scatter.2.cloned.1.call-start = ((), (), s32[]{:S(2)}) async-start(), calls=%async_computation.4 | async-start | bytes 6553600 | tf_op jit(solution)/shard_map/reduce_scatter | solution.py:49
  128.1 4.6 %copy-start.2 = (bf16[1,2048,896]{2,1,0:T(8,128)(2,1)S(1)}, bf16[1,2048,896]{2,1,0:T(8,128)(2,1)}, u32[]{:S(2)}) copy-start(bf16[1,2048,896]{2,1,0:T(8,128)(2,1)} %param.11) | copy-start | bytes 11010052
  130.4 2.3 copy-start
  157.4 54.9 %copy-start.1 = (f32[256,2]{0,1:T(2,128)S(1)}, f32[256,2]{0,1:T(2,128)}, u32[]{:S(2)}) copy-start(f32[256,2]{0,1:T(2,128)} %param.10) | copy-start | bytes 6148
  206.8 36.7 %all-to-all-start.2 = ((bf16[8,160,512]{2,1,0:T(8,128)(2,1)}), bf16[8,160,512]{2,1,0:T(8,128)(2,1)S(1)}, u32[]{:S(2)}, u32[]{:S(2)}) async-start(bf16[8,160,512]{2,1,0:T(8,128)(2,1)} %bitcast.47), calls=%async_computation.3 | async-start | bytes 2621440 | tf_op jit(solution)/shard_map/all_to_all | solution.py:52
Sparse Core Ops, SparseCore 0:
  157.5 49.2 reduce-scatter.1
